TPU v7x, 32 devices: a whole 2x2x4 slice. The times are simulated.
32 devices in a mesh: rep: 2 (over y), fs: 4 (over z), tp: 4 (over x, core).
Axes of the slice: x: 2, y: 2, z: 4, core: 2. Of those that a mesh axis runs over, the one named last changes fastest.
Arguments:
- tokens: bfloat16 [8, 512, 2048], P(('rep', 'fs')), may hold values from -6 to 6
- first_gain: float32 [2048], replicated, may hold values from 0.1 to 1.9
- in_matrix: float32 [2048, 2048], P('fs', 'tp'), may hold values from -0.125 to 0.125
- in_scale: float32 [2048], P('tp'), may hold values from 0.5 to 2
- conv_taps: float32 [4, 2048], P(None, 'tp'), may hold values from -3 to 3
- decay_rate: float32 [2, 2048], P(None, 'tp'), may hold values from 0 to 1, as said below
- recall_maps: float32 [2, 8, 256, 256], P(None, 'tp'), may hold values from -0.375 to 0.375
- admit_maps: float32 [2, 8, 256, 256], P(None, 'tp'), may hold values from -0.375 to 0.375
- out_matrix: float32 [2048, 2048], P('fs', 'tp'), may hold values from -0.125 to 0.125
- out_scale: float32 [2048], P('fs'), may hold values from 0.5 to 2
- second_gain: float32 [2048], replicated, may hold values from 0.1 to 1.9
- up_matrix: float32 [2048, 4096], P('fs', 'tp'), may hold values from -0.125 to 0.125
- up_scale: float32 [4096], P('tp'), may hold values from 0.5 to 2
- down_matrix: float32 [2048, 4096], P('fs', 'tp'), may hold values from -0.09375 to 0.09375
- down_scale: float32 [2048], P('fs'), may hold values from 0.5 to 2
Outputs:
- layer_out: bfloat16 [8, 512, 2048], P(('rep', 'fs'))
Inputs may be any that keep to these rules, and one draw needn't show every extreme that they name: `decay_rate`: positive per-step decay rates.
All inputs are finite; a program needn't handle non-finite values.
Results may differ from a plain program's by a relative error of at most 0.024.
Values may be sent and summed in bfloat16 or wider, within the bound.
No kernel may reach another device: no remote copies, remote signals or barrier semaphores. Data moves between devices by JAX's collectives and lax.ppermute only.
A program may use at most 64 MiB of HBM per device.

v0:
```python
import jax
import jax.numpy as jnp
from jax import lax
from jax.sharding import PartitionSpec as P

EPSILON = 1e-06
RATE_GAIN = 8.0


def normalize(stream, gain):
    return stream * lax.rsqrt(jnp.mean(stream * stream, axis=-1, keepdims=True) + EPSILON) * gain


def convolve(values, taps):
    length = values.shape[0]
    count = taps.shape[0]
    padded = jnp.pad(values, ((count // 2, count - 1 - count // 2), (0, 0)))
    total = taps[0] * padded[0:length]
    for offset in range(1, count):
        total = total + taps[offset] * padded[offset : offset + length]
    return total


def block_map(values, maps):
    length = values.shape[0]
    count, width = (maps.shape[0], maps.shape[1])
    grouped = values.reshape(length, count, width)
    mapped = jnp.einsum("lnj,njk->lnk", grouped, maps, precision=lax.Precision.HIGHEST)
    return mapped.reshape(length, count * width)


def combine_steps(earlier, later):
    return (earlier[0] * later[0], later[0] * earlier[1] + later[1])


def one_direction(values, rate, recall_map, admit_map):
    recall = jax.nn.sigmoid(block_map(values, recall_map))
    admit = jax.nn.sigmoid(block_map(values, admit_map))
    log_decay = -RATE_GAIN * recall * rate
    decay = jnp.exp(log_decay)
    drive = jnp.sqrt(-jnp.expm1(2.0 * log_decay)) * admit * values
    carried = lax.associative_scan(combine_steps, (decay, drive), axis=0)
    return carried[1]


def recurrence(values, rates, recall_maps, admit_maps):
    forward = one_direction(values, rates[0], recall_maps[0], admit_maps[0])
    backward = one_direction(values[::-1], rates[1], recall_maps[1], admit_maps[1])[::-1]
    return forward + backward


def contract_last(left, right):
    return lax.dot_general(
        left, right, (((1,), (1,)), ((), ())), preferred_element_type=jnp.float32
    )


def body(
    tokens,
    first_gain,
    in_matrix,
    in_scale,
    conv_taps,
    decay_rate,
    recall_maps,
    admit_maps,
    out_matrix,
    out_scale,
    second_gain,
    up_matrix,
    up_scale,
    down_matrix,
    down_scale,
):
    stream = tokens.reshape(tokens.shape[1], tokens.shape[2]).astype(jnp.float32)
    in_cols, out_rows, out_factor, down_factor = (
        lax.all_gather(in_matrix.astype(jnp.bfloat16), "fs", axis=0, tiled=True),
        lax.all_gather(out_matrix.astype(jnp.bfloat16), "fs", axis=0, tiled=True),
        lax.all_gather(out_scale.astype(jnp.bfloat16), "fs", axis=0, tiled=True),
        lax.all_gather(down_scale.astype(jnp.bfloat16), "fs", axis=0, tiled=True),
    )
    normed = normalize(stream, first_gain).astype(jnp.bfloat16)
    before = (
        jnp.dot(normed, in_cols, preferred_element_type=jnp.float32) * in_scale.astype(jnp.bfloat16)
    ).astype(jnp.bfloat16)
    conv_out = convolve(before.astype(jnp.float32), conv_taps)
    mixed = recurrence(conv_out, decay_rate, recall_maps, admit_maps).astype(jnp.bfloat16)
    partial_value = contract_last(mixed, out_rows)
    middle = stream + out_factor * lax.psum(partial_value.astype(jnp.bfloat16), "tp").astype(
        jnp.float32
    )
    second_normed = normalize(middle, second_gain).astype(jnp.bfloat16)
    raised = jnp.dot(
        second_normed,
        lax.all_gather(up_matrix.astype(jnp.bfloat16), "fs", axis=0, tiled=True),
        preferred_element_type=jnp.float32,
    )
    active = jnp.square(jax.nn.relu(raised * up_scale.astype(jnp.bfloat16))).astype(jnp.bfloat16)
    lowered = contract_last(
        active, lax.all_gather(down_matrix.astype(jnp.bfloat16), "fs", axis=0, tiled=True)
    )
    result = (
        middle + down_factor * lax.psum(lowered.astype(jnp.bfloat16), "tp").astype(jnp.float32)
    ).astype(jnp.bfloat16)
    return result.reshape(tokens.shape)


def solution(mesh):
    placed = (
        P(("rep", "fs"), None, None),
        P(),
        P("fs", "tp"),
        P("tp"),
        P(None, "tp"),
        P(None, "tp"),
        P(None, "tp", None, None),
        P(None, "tp", None, None),
        P("fs", "tp"),
        P("fs"),
        P(),
        P("fs", "tp"),
        P("tp"),
        P("fs", "tp"),
        P("fs"),
    )
    return jax.shard_map(
        body, mesh=mesh, in_specs=placed, out_specs=P(("rep", "fs"), None, None), check_vma=False
    )
```

profile of v0, /device:TPU:0, one launch (start us, length us, event | category | flops | bytes accessed | tf_op | source)
XLA Modules:
  0.0 626.4 jit_solution(6509741155508411147)
XLA Ops:
  6.5 2.2 convert_element_type.82
  11.0 46.4 %all-gather.7.cloned.1.call-done = bf16[2048,512]{1,0:T(8,128)(2,1)} async-done(((bf16[512,512]{1,0:T(8,128)(2,1)}), bf16[2048,512]{1,0:T(8,128)(2,1)}) %all-gather.7.cloned.1.call-update) | async-done | bytes 2097168 | tf_op jit(solution)/shard_map/all_gather | solution.py:77
  57.3 2.9 fusion.32
  62.2 2.3 fusion.28
  64.6 2.6 copy.40
  67.2 3.3 fusion.25
  70.5 2.6 copy.41
  73.0 5.3 multiply_exponential_fusion.1
  78.3 2.1 slice.467
  80.4 2.1 slice.468
  82.5 3.7 slice.466
  86.1 3.7 slice.470
  89.8 2.7 fusion.73
  92.5 2.5 slice.473
  95.0 2.5 slice.474
  97.5 2.5 slice.472
  100.0 2.5 slice.476
  102.5 2.0 fusion.75
  107.5 1.6 slice.482
  109.1 1.8 fusion.77
  158.1 1.6 slice.477
  161.0 2.5 slice.528
  163.6 2.5 slice.471
  167.4 2.1 slice.530
  169.5 3.7 slice.465
  173.8 6.8 %rev.6 = f32[512,512]{1,0:T(8,128)S(1)} reverse(f32[512,512]{1,0:T(8,128)} %copy-done.4), dimensions={0} | reverse | bytes 2097152 | tf_op jit(solution)/shard_map/rev | solution.py:48
  180.6 3.7 fusion.22
  184.3 2.3 fusion.19
  186.6 2.6 copy.42
  190.5 3.6 multiply_exponential_fusion
  194.1 2.1 slice.537
  196.2 2.1 slice.538
  198.2 3.6 slice.536
  201.9 3.6 slice.540
  205.5 2.7 fusion.74
  208.2 2.5 slice.543
  210.7 2.5 slice.544
  213.2 2.5 slice.542
  215.7 2.5 slice.546
  218.2 2.0 fusion.76
  224.8 1.8 fusion.78
  270.5 1.6 slice.547
  273.5 1.9 slice.598
  275.4 2.5 slice.541
  279.3 2.1 slice.600
  281.4 3.7 slice.535
  298.7 4.6 pad.132
  304.9 2.7 pad.131
  315.7 4.6 pad.150
  321.8 2.7 pad.149
  324.5 2.8 add.359
  327.3 9.0 %rev.7 = f32[512,512]{1,0:T(8,128)} reverse(f32[512,512]{1,0:T(8,128)} %add.359), dimensions={0} | reverse | bytes 2097152 | tf_op jit(solution)/shard_map/rev | solution.py:48
  336.3 4.9 convolution_convert_fusion.1
  341.2 2.8 convert_element_type.94
  344.1 2.9 convert_element_type.98
  347.1 11.9 %all-gather = bf16[4,1,512]{2,1,0:T(2,128)(2,1)S(1)} all-gather(bf16[1,1,512]{2,1,0:T(2,128)(2,1)S(1)} %reshape.72), channel_id=1, replica_groups=mesh['rep'=2,'fs'=4,'tp'=4] {'fs'}, dimensions={0}, use_global_device_ids=true | all-gather | bytes 5120 | tf_op jit(solution)/shard_map/all_gather | solution.py:79
  359.1 32.4 %all-reduce.40.cloned.1.call-done = bf16[512,2048]{1,0:T(8,128)(2,1)} async-done(((bf16[512,2048]{1,0:T(8,128)(2,1)}), bf16[512,2048]{1,0:T(8,128)(2,1)}) %all-reduce.40.cloned.1.call-update) | async-done | bytes 2097168 | tf_op jit(solution)/shard_map/psum | solution.py:89
  391.5 2.5 multiply_reduce_fusion
  394.0 79.8 %all-gather.11.cloned.1.call-done = bf16[2048,1024]{1,0:T(8,128)(2,1)} async-done(((bf16[512,1024]{1,0:T(8,128)(2,1)}), bf16[2048,1024]{1,0:T(8,128)(2,1)}) %all-gather.11.cloned.1.call-update) | async-done | bytes 4194320 | tf_op jit(solution)/shard_map/all_gather | solution.py:95
  473.8 80.7 %all-gather.13.cloned.1.call-done = bf16[2048,1024]{1,0:T(8,128)(2,1)} async-done(((bf16[512,1024]{1,0:T(8,128)(2,1)}), bf16[2048,1024]{1,0:T(8,128)(2,1)}) %all-gather.13.cloned.1.call-update) | async-done | bytes 4194320 | tf_op jit(solution)/shard_map/all_gather | solution.py:100
  554.4 9.9 %convolution_convert_fusion = bf16[512,2048]{1,0:T(8,128)(2,1)} fusion(bf16[2048,1024]{1,0:T(8,128)(2,1)} %all-gather.13.cloned.1.call-done, bf16[2048,1024]{1,0:T(8,128)(2,1)} %all-gather.11.cloned.1.call-done, bf16[512,2048]{1,0:T(8,128)(2,1)} %all-reduce.40.cloned.1.call-done, bf16[1,512,2048]{2,1,0:T(8,128)(2,1)S(1)} %copy-done, ...), kind=kOutput, calls=%fused_computation.9 | convolution fusion | flops 4305453056 | bytes 14702592 | tf_op jit(solution)/shard_map/dot_general | solution.py:53
  565.1 11.9 %all-gather.1 = bf16[4,1,512]{2,1,0:T(2,128)(2,1)S(1)} all-gather(bf16[1,1,512]{2,1,0:T(2,128)(2,1)S(1)} %reshape.74), channel_id=1, replica_groups=mesh['rep'=2,'fs'=4,'tp'=4] {'fs'}, dimensions={0}, use_global_device_ids=true | all-gather | bytes 5120 | tf_op jit(solution)/shard_map/all_gather | solution.py:80
  577.0 37.4 %all-reduce.42.cloned.1.call-done = bf16[512,2048]{1,0:T(8,128)(2,1)} async-done(((bf16[512,2048]{1,0:T(8,128)(2,1)}), bf16[512,2048]{1,0:T(8,128)(2,1)}) %all-reduce.42.cloned.1.call-update) | async-done | bytes 2097168 | tf_op jit(solution)/shard_map/psum | solution.py:103
  614.4 5.1 fusion.4
  (277 shorter events, 135.1 us)
Async XLA Ops:
  6.5 2.4 copy-start.8
  6.5 3.3 copy-start.31
  6.5 3.3 copy-start
  6.5 50.8 %all-gather.7.cloned.1.call-start = ((), (), s32[]{:S(2)}) async-start(), calls=%async_computation | async-start | bytes 2621440 | tf_op jit(solution)/shard_map/all_gather | solution.py:77
  8.8 1.5 copy-start.32
  8.8 2.1 copy-start.36
  8.8 48.5 %copy-start.39 = (f32[2048]{0:T(1024)S(1)}, f32[2048]{0:T(1024)}, u32[]{:S(2)}) copy-start(f32[2048]{0:T(1024)} %param.16) | copy-start | bytes 24580
  8.8 327.4 %all-gather.9.cloned.1.call-start = ((), (), s32[]{:S(2)}) async-start(), calls=%async_computation.1 | async-start | bytes 2621440 | tf_op jit(solution)/shard_map/all_gather | solution.py:78
  9.8 381.7 %all-reduce.40.cloned.1.call-start = ((), (), s32[]{:S(2)}) async-start(), calls=%async_computation.2 | async-start | bytes 4194304 | tf_op jit(solution)/shard_map/psum | solution.py:89
  60.2 4.3 copy-start.2
  60.2 2.0 copy-start.37
  60.7 6.5 %copy-start.4 = (f32[512,512]{1,0:T(8,128)}, f32[512,512]{1,0:T(8,128)S(1)}, u32[]{:S(2)}) copy-start(f32[512,512]{1,0:T(8,128)S(1)} %multiply_add_fusion) | copy-start | bytes 3145732
  180.6 3.7 copy-start.3
  180.6 3.7 copy-start.38
  186.6 2.6 copy-start.9
  186.6 3.9 copy-start.28
  266.4 22.1 %copy-start.13 = (f32[7,512]{1,0:T(8,128)S(1)}, f32[7,512]{1,0:T(8,128)}, u32[]{:S(2)}) copy-start(f32[7,512]{1,0:T(8,128)} %slice.495) | copy-start | bytes 43012
  281.4 13.4 %copy-start.10 = (f32[63,512]{1,0:T(8,128)S(1)}, f32[63,512]{1,0:T(8,128)}, u32[]{:S(2)}) copy-start(f32[63,512]{1,0:T(8,128)} %slice.477) | copy-start | bytes 387076
  289.2 6.5 %copy-start.25 = (f32[1,512]{1,0:T(1,128)S(1)}, f32[1,512]{1,0:T(1,128)}, u32[]{:S(2)}) copy-start(f32[1,512]{1,0:T(1,128)} %slice.603) | copy-start | bytes 6148
  289.9 6.6 %copy-start.5 = (f32[127,512]{1,0:T(8,128)S(1)}, f32[127,512]{1,0:T(8,128)}, u32[]{:S(2)}) copy-start(f32[127,512]{1,0:T(8,128)} %slice.528) | copy-start | bytes 780292
  289.9 6.6 %copy-start.6 = (f32[127,512]{1,0:T(8,128)S(1)}, f32[127,512]{1,0:T(8,128)}, u32[]{:S(2)}) copy-start(f32[127,512]{1,0:T(8,128)} %slice.471) | copy-start | bytes 780292
  293.1 3.5 copy-start.24
  298.7 6.1 copy-start.23
  303.3 4.4 copy-start.16
  303.3 5.2 copy-start.17
  304.8 2.9 copy-start.19
  304.8 2.9 copy-start.20
  304.8 2.9 copy-start.21
  304.8 2.9 copy-start.22
  304.8 3.7 copy-start.18
  304.8 3.7 copy-start.30
  304.8 3.8 copy-start.14
  304.8 3.8 copy-start.15
  304.8 3.8 copy-start.29
  304.9 7.1 %copy-start.11 = (f32[63,512]{1,0:T(8,128)S(1)}, f32[63,512]{1,0:T(8,128)}, u32[]{:S(2)}) copy-start(f32[63,512]{1,0:T(8,128)} %slice.547) | copy-start | bytes 387076
  304.9 7.1 %copy-start.12 = (f32[63,512]{1,0:T(8,128)S(1)}, f32[63,512]{1,0:T(8,128)}, u32[]{:S(2)}) copy-start(f32[63,512]{1,0:T(8,128)} %slice.596) | copy-start | bytes 387076
  308.7 4.8 copy-start.7
  311.9 1.7 copy-start.27
  315.7 6.1 copy-start.26
  324.5 11.8 %copy-start.1 = (f32[512,512]{1,0:T(8,128)S(1)}, f32[512,512]{1,0:T(8,128)}, u32[]{:S(2)}) copy-start(f32[512,512]{1,0:T(8,128)} %pad.132) | copy-start | bytes 3145732
  341.1 132.6 %all-gather.11.cloned.1.call-start = ((), (), s32[]{:S(2)}) async-start(), calls=%async_computation.3 | async-start | bytes 5242880 | tf_op jit(solution)/shard_map/all_gather | solution.py:95
  344.0 3.1 copy-start.34
  344.0 15.1 %copy-start.33 = (f32[1024]{0:T(1024)S(1)}, f32[1024]{0:T(1024)}, u32[]{:S(2)}) copy-start(f32[1024]{0:T(1024)} %param.27) | copy-start | bytes 12292
  344.0 210.4 %all-gather.13.cloned.1.call-start = ((), (), s32[]{:S(2)}) async-start(), calls=%async_computation.4 | async-start | bytes 5242880 | tf_op jit(solution)/shard_map/all_gather | solution.py:100
  347.0 267.4 %all-reduce.42.cloned.1.call-start = ((), (), s32[]{:S(2)}) async-start(), calls=%async_computation.5 | async-start | bytes 4194304 | tf_op jit(solution)/shard_map/psum | solution.py:103
  391.5 163.0 %copy-start.40 = (f32[2048]{0:T(1024)S(1)}, f32[2048]{0:T(1024)}, u32[]{:S(2)}) copy-start(f32[2048]{0:T(1024)} %param.25) | copy-start | bytes 24580
  564.4 0.7 copy-start.35
Sparse Core Ops, SparseCore 0:
  8.9 48.3 all-gather.6
  58.9 44.4 all-gather.8
  341.3 50.1 all-reduce.39
  392.9 80.8 all-gather.10
  475.2 79.2 all-gather.12
  564.5 49.8 all-reduce.41
where the time goes:
time: 633 us; the launch traced here: 626 us
  waiting for transfers between devices  277 us (44%)
  local copies, waits for them, and re-layouts  205 us (32%)
  other arithmetic  76.6 us (12%)
  matrix products  29.3 us (5%)
  blocking collectives  23.9 us (4%)
  between operations  14.3 us (2%)
    slice x106, local copies, waits for them, and re-layouts, one_direction(): carried = lax.associative_scan(combine_steps, (decay, drive), axis=0)  159 us
    all_gather x1, waiting for transfers between devices, body(): lax.all_gather(down_matrix.astype(jnp.bfloat16), 'fs', axis=0, tiled=True)  80.7 us
    all_gather x1, waiting for transfers between devices, body(): lax.all_gather(up_matrix.astype(jnp.bfloat16), 'fs', axis=0, tiled=True)  79.8 us
    all_gather x1, waiting for transfers between devices, body(): lax.all_gather(in_matrix.astype(jnp.bfloat16), 'fs', axis=0, tiled=True)  46.4 us
    psum x1, waiting for transfers between devices, body(): lax.psum(lowered.astype(jnp.bfloat16), 'tp').astype(jnp.float32)  37.4 us
    psum x1, waiting for transfers between devices, body(): lax.psum(partial_value.astype(jnp.bfloat16), 'tp').astype(jnp.float32)  32.4 us
    mul x14, other arithmetic, combine_steps(): return (earlier[0] * later[0], later[0] * earlier[1] + later[1])  24.4 us
    pad x32, local copies, waits for them, and re-layouts, one_direction(): carried = lax.associative_scan(combine_steps, (decay, drive), axis=0)  18.9 us
  transfers between devices with their start and end apart: 6, of which 5 were waited for; matrix products, arithmetic and copies ran while one was open for 46% of the time, Pallas kernels for 0%

commit v1 on v0

--- a/solution.py
+++ b/solution.py
@@ -1,6 +1,8 @@
 import jax
 import jax.numpy as jnp
 from jax import lax
+from jax.experimental import pallas as pl
+from jax.experimental.pallas import tpu as pltpu
 from jax.sharding import PartitionSpec as P
 
 EPSILON = 1e-06
@@ -11,42 +13,123 @@
     return stream * lax.rsqrt(jnp.mean(stream * stream, axis=-1, keepdims=True) + EPSILON) * gain
 
 
-def convolve(values, taps):
-    length = values.shape[0]
+SEGMENTS = 8
+LANES = 128
+
+
+def one_minus_exp(y):
+    series = -y * (1.0 + y * (1.0 / 2) * (1.0 + y * (1.0 / 3) * (1.0 + y * 0.25 * (1.0 + y * 0.2))))
+    return jnp.where(y > -0.25, series, 1.0 - jnp.exp(y))
+
+
+def sigmoid(x):
+    return 1.0 / (1.0 + jnp.exp(-x))
+
+
+def recurrence_kernel(before, taps, rates, recall_maps, admit_maps, mixed, padded, hi, lo, decay, drive, states):
+    length, width = before.shape
     count = taps.shape[0]
-    padded = jnp.pad(values, ((count // 2, count - 1 - count // 2), (0, 0)))
-    total = taps[0] * padded[0:length]
-    for offset in range(1, count):
-        total = total + taps[offset] * padded[offset : offset + length]
-    return total
-
-
-def block_map(values, maps):
-    length = values.shape[0]
-    count, width = (maps.shape[0], maps.shape[1])
-    grouped = values.reshape(length, count, width)
-    mapped = jnp.einsum("lnj,njk->lnk", grouped, maps, precision=lax.Precision.HIGHEST)
-    return mapped.reshape(length, count * width)
-
-
-def combine_steps(earlier, later):
-    return (earlier[0] * later[0], later[0] * earlier[1] + later[1])
-
-
-def one_direction(values, rate, recall_map, admit_map):
-    recall = jax.nn.sigmoid(block_map(values, recall_map))
-    admit = jax.nn.sigmoid(block_map(values, admit_map))
-    log_decay = -RATE_GAIN * recall * rate
-    decay = jnp.exp(log_decay)
-    drive = jnp.sqrt(-jnp.expm1(2.0 * log_decay)) * admit * values
-    carried = lax.associative_scan(combine_steps, (decay, drive), axis=0)
-    return carried[1]
-
-
-def recurrence(values, rates, recall_maps, admit_maps):
-    forward = one_direction(values, rates[0], recall_maps[0], admit_maps[0])
-    backward = one_direction(values[::-1], rates[1], recall_maps[1], admit_maps[1])[::-1]
-    return forward + backward
+    front = 8
+    tiles = width // LANES
+    padded[pl.ds(0, front), :] = jnp.zeros((front, width), jnp.float32)
+    padded[pl.ds(front, length), :] = before[...].astype(jnp.float32)
+    padded[pl.ds(front + length, 8), :] = jnp.zeros((8, width), jnp.float32)
+    for slot in range(4):
+        source = (recall_maps, admit_maps)[slot % 2]
+        values = source[slot // 2, 0]
+        top = values.astype(jnp.bfloat16)
+        hi[:, slot * width : (slot + 1) * width] = top
+        lo[:, slot * width : (slot + 1) * width] = (values - top.astype(jnp.float32)).astype(jnp.bfloat16)
+    rows = min(128, length)
+    for start in range(0, length, rows):
+        total = taps[0:1, :] * padded[pl.ds(front + start - count // 2, rows), :]
+        for offset in range(1, count):
+            total = total + taps[offset : offset + 1, :] * padded[pl.ds(front + start + offset - count // 2, rows), :]
+        top = total.astype(jnp.bfloat16)
+        rest = (total - top.astype(jnp.float32)).astype(jnp.bfloat16)
+        for direction in range(2):
+            span = slice(direction * 2 * width, (direction + 1) * 2 * width)
+            gates = (
+                jnp.dot(top, hi[:, span], preferred_element_type=jnp.float32)
+                + jnp.dot(rest, hi[:, span], preferred_element_type=jnp.float32)
+                + jnp.dot(top, lo[:, span], preferred_element_type=jnp.float32)
+            )
+            recall = sigmoid(gates[:, :width])
+            admit = sigmoid(gates[:, width:])
+            log_decay = (-RATE_GAIN * rates[direction : direction + 1, :]) * recall
+            step_decay = jnp.exp(log_decay)
+            step_drive = jnp.sqrt(one_minus_exp(2.0 * log_decay)) * admit * total
+            for tile in range(tiles):
+                lanes = slice(tile * LANES, (tile + 1) * LANES)
+                decay[direction * tiles + tile, pl.ds(start, rows), :] = step_decay[:, lanes]
+                drive[direction * tiles + tile, pl.ds(start, rows), :] = step_drive[:, lanes]
+    step = length // SEGMENTS
+    zero = jnp.zeros((SEGMENTS, LANES), jnp.float32)
+    one = jnp.ones((SEGMENTS, LANES), jnp.float32)
+
+    def picked(ref, lane, i):
+        at = i if lane < tiles else step - 1 - i
+        return ref[lane, pl.ds(at, SEGMENTS, stride=step), :]
+
+    def first_pass(i, carry):
+        after = []
+        for lane, (state, product) in enumerate(carry):
+            a = picked(decay, lane, i)
+            after.append((a * state + picked(drive, lane, i), a * product))
+        return tuple(after)
+
+    ends = lax.fori_loop(0, step, first_pass, ((zero, one),) * (2 * tiles), unroll=8)
+    begins = []
+    for lane, (state, product) in enumerate(ends):
+        row = zero[0:1]
+        rows_of = [row]
+        order = range(SEGMENTS - 1) if lane < tiles else range(SEGMENTS - 1, 0, -1)
+        for s in order:
+            row = state[s : s + 1] + product[s : s + 1] * row
+            rows_of.append(row)
+        begins.append(jnp.concatenate(rows_of if lane < tiles else rows_of[::-1], axis=0))
+
+    def second_pass(i, carry):
+        after = []
+        for lane, state in enumerate(carry):
+            state = picked(decay, lane, i) * state + picked(drive, lane, i)
+            at = i if lane < tiles else step - 1 - i
+            states[lane, pl.ds(at, SEGMENTS, stride=step), :] = state
+            after.append(state)
+        return tuple(after)
+
+    lax.fori_loop(0, step, second_pass, tuple(begins), unroll=8)
+    for tile in range(tiles):
+        mixed[:, tile * LANES : (tile + 1) * LANES] = (states[tile] + states[tiles + tile]).astype(jnp.bfloat16)
+
+
+def recurrence(before, taps, rates, recall_maps, admit_maps):
+    length, channels = before.shape
+    groups, width = recall_maps.shape[1:3]
+    column = lambda g: (0, g)
+    return pl.pallas_call(
+        recurrence_kernel,
+        grid=(groups,),
+        in_specs=[
+            pl.BlockSpec((length, width), column),
+            pl.BlockSpec((taps.shape[0], width), column),
+            pl.BlockSpec((2, width), column),
+            pl.BlockSpec((2, 1, width, width), lambda g: (0, g, 0, 0)),
+            pl.BlockSpec((2, 1, width, width), lambda g: (0, g, 0, 0)),
+        ],
+        out_specs=pl.BlockSpec((length, width), column),
+        out_shape=jax.ShapeDtypeStruct((length, channels), jnp.bfloat16),
+        scratch_shapes=[
+            pltpu.VMEM((length + 16, width), jnp.float32),
+            pltpu.VMEM((width, 4 * width), jnp.bfloat16),
+            pltpu.VMEM((width, 4 * width), jnp.bfloat16),
+            pltpu.VMEM((2 * width // LANES, length, LANES), jnp.float32),
+            pltpu.VMEM((2 * width // LANES, length, LANES), jnp.float32),
+            pltpu.VMEM((2 * width // LANES, length, LANES), jnp.float32),
+        ],
+        compiler_params=pltpu.CompilerParams(dimension_semantics=("arbitrary",)),
+        name="recurrence",
+    )(before, taps, rates, recall_maps, admit_maps)
 
 
 def contract_last(left, right):
@@ -83,8 +166,7 @@
     before = (
         jnp.dot(normed, in_cols, preferred_element_type=jnp.float32) * in_scale.astype(jnp.bfloat16)
     ).astype(jnp.bfloat16)
-    conv_out = convolve(before.astype(jnp.float32), conv_taps)
-    mixed = recurrence(conv_out, decay_rate, recall_maps, admit_maps).astype(jnp.bfloat16)
+    mixed = recurrence(before, conv_taps, decay_rate, recall_maps, admit_maps)
     partial_value = contract_last(mixed, out_rows)
     middle = stream + out_factor * lax.psum(partial_value.astype(jnp.bfloat16), "tp").astype(
         jnp.float32

time: 633 us -> 393 us (0.62); the launches traced: 626 us -> 393 us
  local copies, waits for them, and re-layouts: 205 us -> 0.71 us
  other arithmetic: 76.6 us -> 16.8 us
  waiting for transfers between devices: 277 us -> 307 us
  Pallas kernels: 0 us -> 13 us
  matrix products: 29.3 us -> 18 us
    slice x107 -> x0, local copies, waits for them, and re-layouts: 159 us -> none  [the longest x106 159 us: one_direction(): carried = lax.associative_scan(combine_steps, (decay, drive), axis=0)]
    all_gather x1, waiting for transfers between devices: 0.01 us -> 29.4 us  [body(): lax.all_gather(out_matrix.astype(jnp.bfloat16), 'fs', axis=0, tiled=True)]
    mul x15 -> x0, other arithmetic: 25 us -> none  [the longest x14 24.4 us: combine_steps(): return (earlier[0] * later[0], later[0] * earlier[1] + later[1])]
    pad x32 -> x0, local copies, waits for them, and re-layouts: 18.9 us -> none  [one_direction(): carried = lax.associative_scan(combine_steps, (decay, drive), axis=0)]
    add x36 -> x0, other arithmetic: 18.2 us -> none  [the longest x18 10.4 us: combine_steps(): return (earlier[0] * later[0], later[0] * earlier[1] + later[1])]
    rev x2 -> x0, local copies, waits for them, and re-layouts: 15.8 us -> none  [the longest x1 8.95 us: recurrence(): one_direction(values[::-1], rates[1], recall_maps[1], admit_maps[1])[::-1]]
    pallas_call x0 -> x1, Pallas kernels: none -> 13 us  [recurrence(): pl.pallas_call(recurrence_kernel, grid=(groups,), in_specs=[pl.BlockSpec(...]
    dot_general x4 -> x0, matrix products: 11.6 us -> none  [block_map(): jnp.einsum('lnj,njk->lnk', grouped, maps, precision=lax.Precision.HIGHEST)]
  transfers between devices with their start and end apart: 6 -> 6, of which waited for: 5 -> 6; matrix products, arithmetic and copies ran while one was open for 46% -> 3% of each run, Pallas kernels for 0% -> 3%
where the time goes in v1:
time: 393 us
  waiting for transfers between devices  307 us (78%)
  blocking collectives  23.9 us (6%)
  matrix products  18 us (5%)
  other arithmetic  16.8 us (4%)
  between operations  13.6 us (3%)
  Pallas kernels  13 us (3%)
    all_gather x1, waiting for transfers between devices, body(): lax.all_gather(down_matrix.astype(jnp.bfloat16), 'fs', axis=0, tiled=True)  80.7 us
    all_gather x1, waiting for transfers between devices, body(): lax.all_gather(up_matrix.astype(jnp.bfloat16), 'fs', axis=0, tiled=True)  79.8 us
    all_gather x1, waiting for transfers between devices, body(): lax.all_gather(in_matrix.astype(jnp.bfloat16), 'fs', axis=0, tiled=True)  47 us
    psum x1, waiting for transfers between devices, body(): lax.psum(lowered.astype(jnp.bfloat16), 'tp').astype(jnp.float32)  37.4 us
    psum x1, waiting for transfers between devices, body(): lax.psum(partial_value.astype(jnp.bfloat16), 'tp').astype(jnp.float32)  32.5 us
    all_gather x1, waiting for transfers between devices, body(): lax.all_gather(out_matrix.astype(jnp.bfloat16), 'fs', axis=0, tiled=True)  29.4 us
    dot_general x2, matrix products, contract_last(): lax.dot_general(left, right, (((1,), (1,)), ((), ())), preferred_element_...  14.3 us
    pallas_call x1, Pallas kernels, recurrence(): pl.pallas_call(recurrence_kernel, grid=(groups,), in_specs=[pl.BlockSpec(...  13 us
  transfers between devices with their start and end apart: 6, of which 6 were waited for; matrix products, arithmetic and copies ran while one was open for 3% of the time, Pallas kernels for 3%

profile of v1, /device:TPU:0, one launch (start us, length us, event | category | flops | bytes accessed | tf_op | source)
XLA Modules:
  0.0 393.0 jit_solution(4886858611782767147)
XLA Ops:
  6.5 0.0 copy-start.1
  6.5 0.0 copy-start
  6.5 0.0 all-gather.7.cloned.1.call-start
  6.5 2.2 convert_element_type.74
  8.8 0.0 all-gather.7.cloned.1.call-update
  8.8 0.0 copy-start.5
  8.8 0.0 copy-start.6
  8.8 0.0 all-gather.9.cloned.1.call-start
  8.9 0.0 copy-done.1
  8.9 0.9 convert_element_type.78
  9.7 0.0 all-gather.9.cloned.1.call-update
  9.8 0.0 all-reduce.3.cloned.1.call-start
  9.8 0.0 copy-done
  9.8 0.5 fusion
  10.3 0.0 copy-done.5
  10.3 47.0 %all-gather.7.cloned.1.call-done = bf16[2048,512]{1,0:T(8,128)(2,1)} async-done(((bf16[512,512]{1,0:T(8,128)(2,1)}), bf16[2048,512]{1,0:T(8,128)(2,1)}) %all-gather.7.cloned.1.call-update) | async-done | bytes 2097168 | tf_op jit(solution)/shard_map/all_gather | solution.py:160
  57.3 0.0 copy-done.6
  57.3 3.7 fusion.17.before
  61.0 13.0 %recurrence.1 = bf16[512,512]{1,0:T(8,128)(2,1)} custom-call(bf16[512,512]{1,0:T(8,128)(2,1)} %fusion.17.before, f32[4,512]{1,0:T(4,128)} %taps.1, f32[2,512]{1,0:T(2,128)} %rates.1, f32[2,2,256,256]{3,2,1,0:T(8,128)} %recall_maps.1, f32[2,2,256,256]{3,2,1,0:T(8,128)} %admit_maps.1), custom_call_target="tpu_custom_call" | custom-call | tf_op jit(solution)/shard_map/recurrence/pallas_call | solution.py:110
  74.0 29.4 %all-gather.9.cloned.1.call-done = bf16[2048,512]{1,0:T(8,128)(2,1)} async-done(((bf16[512,512]{1,0:T(8,128)(2,1)}), bf16[2048,512]{1,0:T(8,128)(2,1)}) %all-gather.9.cloned.1.call-update) | async-done | bytes 2097168 | tf_op jit(solution)/shard_map/all_gather | solution.py:161
  103.4 4.4 %convolution_convert_fusion.1 = bf16[512,2048]{1,0:T(8,128)(2,1)} fusion(bf16[512,512]{1,0:T(8,128)(2,1)} %recurrence.1, bf16[2048,512]{1,0:T(8,128)(2,1)} %all-gather.9.cloned.1.call-done), kind=kOutput, calls=%fused_computation.10 | convolution fusion | flops 1074790400 | bytes 4718592 | tf_op jit(solution)/shard_map/dot_general | solution.py:136
  107.8 0.0 all-reduce.3.cloned.1.call-update
  107.8 0.0 all-gather.11.cloned.1.call-start
  107.8 2.7 convert_element_type.84
  110.6 0.0 all-gather.11.cloned.1.call-update
  110.6 0.0 copy-start.3
  110.6 0.0 copy-start.2
  110.6 0.0 all-gather.13.cloned.1.call-start
  110.7 2.9 convert_element_type.88
  113.6 0.0 all-gather.13.cloned.1.call-update
  113.6 0.0 all-reduce.5.cloned.1.call-start
  113.6 0.0 copy-done.3
  113.7 11.9 %all-gather = bf16[4,1,512]{2,1,0:T(2,128)(2,1)S(1)} all-gather(bf16[1,1,512]{2,1,0:T(2,128)(2,1)S(1)} %reshape.30), channel_id=1, replica_groups=mesh['rep'=2,'fs'=4,'tp'=4] {'fs'}, dimensions={0}, use_global_device_ids=true | all-gather | bytes 5120 | tf_op jit(solution)/shard_map/all_gather | solution.py:162
  125.6 0.0 copy-done.2
  125.7 32.5 %all-reduce.3.cloned.1.call-done = bf16[512,2048]{1,0:T(8,128)(2,1)} async-done(((bf16[512,2048]{1,0:T(8,128)(2,1)}), bf16[512,2048]{1,0:T(8,128)(2,1)}) %all-reduce.3.cloned.1.call-update) | async-done | bytes 2097168 | tf_op jit(solution)/shard_map/psum | solution.py:171
  158.1 0.0 copy-start.7
  158.1 2.5 multiply_reduce_fusion
  160.6 79.8 %all-gather.11.cloned.1.call-done = bf16[2048,1024]{1,0:T(8,128)(2,1)} async-done(((bf16[512,1024]{1,0:T(8,128)(2,1)}), bf16[2048,1024]{1,0:T(8,128)(2,1)}) %all-gather.11.cloned.1.call-update) | async-done | bytes 4194320 | tf_op jit(solution)/shard_map/all_gather | solution.py:177
  240.4 80.7 %all-gather.13.cloned.1.call-done = bf16[2048,1024]{1,0:T(8,128)(2,1)} async-done(((bf16[512,1024]{1,0:T(8,128)(2,1)}), bf16[2048,1024]{1,0:T(8,128)(2,1)}) %all-gather.13.cloned.1.call-update) | async-done | bytes 4194320 | tf_op jit(solution)/shard_map/all_gather | solution.py:182
  321.1 0.0 copy-done.7
  321.1 9.9 %convolution_convert_fusion = bf16[512,2048]{1,0:T(8,128)(2,1)} fusion(bf16[2048,1024]{1,0:T(8,128)(2,1)} %all-gather.13.cloned.1.call-done, bf16[2048,1024]{1,0:T(8,128)(2,1)} %all-gather.11.cloned.1.call-done, bf16[512,2048]{1,0:T(8,128)(2,1)} %all-reduce.3.cloned.1.call-done, bf16[1,512,2048]{2,1,0:T(8,128)(2,1)S(1)} %copy-done, f32[2048]{0:T(1024)S(1)} %copy-done.7, ...), kind=kOutput, calls=%fused_computation.9 | convolution fusion | flops 4305453056 | bytes 14702592 | tf_op jit(solution)/shard_map/dot_general | solution.py:136
  331.0 0.0 copy-start.4
  331.0 0.0 all-reduce.5.cloned.1.call-update
  331.1 0.7 copy-done.4
  331.7 11.9 %all-gather.1 = bf16[4,1,512]{2,1,0:T(2,128)(2,1)S(1)} all-gather(bf16[1,1,512]{2,1,0:T(2,128)(2,1)S(1)} %reshape.32), channel_id=1, replica_groups=mesh['rep'=2,'fs'=4,'tp'=4] {'fs'}, dimensions={0}, use_global_device_ids=true | all-gather | bytes 5120 | tf_op jit(solution)/shard_map/all_gather | solution.py:163
  343.7 37.4 %all-reduce.5.cloned.1.call-done = bf16[512,2048]{1,0:T(8,128)(2,1)} async-done(((bf16[512,2048]{1,0:T(8,128)(2,1)}), bf16[512,2048]{1,0:T(8,128)(2,1)}) %all-reduce.5.cloned.1.call-update) | async-done | bytes 2097168 | tf_op jit(solution)/shard_map/psum | solution.py:185
  381.1 5.1 %fusion.4 = bf16[1,512,2048]{2,1,0:T(8,128)(2,1)} fusion(bf16[512,2048]{1,0:T(8,128)(2,1)} %all-reduce.5.cloned.1.call-done, bf16[512,2048]{1,0:T(8,128)(2,1)} %all-reduce.3.cloned.1.call-done, bf16[1,512,2048]{2,1,0:T(8,128)(2,1)S(1)} %copy-done, f32[2048]{0:T(1024)S(1)} %bitcast.33, f32[2048]{0:T(1024)S(1)} %bitcast.32), kind=kLoop, calls=%fused_computation.12 | loop fusion | flops 8388608 | bytes 8404992 | tf_op jit(solution)/shard_map/reshape | solution.py:187
  (9 shorter events, 0.1 us)
Async XLA Ops:
  6.5 2.3 copy-start.1
  6.5 3.3 copy-start
  6.5 50.8 %all-gather.7.cloned.1.call-start = ((), (), s32[]{:S(2)}) async-start(), calls=%async_computation | async-start | bytes 2621440 | tf_op jit(solution)/shard_map/all_gather | solution.py:160
  8.8 1.5 copy-start.5
  8.8 48.5 %copy-start.6 = (f32[2048]{0:T(1024)S(1)}, f32[2048]{0:T(1024)}, u32[]{:S(2)}) copy-start(f32[2048]{0:T(1024)} %param.16) | copy-start | bytes 24580
  8.8 94.6 %all-gather.9.cloned.1.call-start = ((), (), s32[]{:S(2)}) async-start(), calls=%async_computation.1 | async-start | bytes 2621440 | tf_op jit(solution)/shard_map/all_gather | solution.py:161
  9.8 148.4 %all-reduce.3.cloned.1.call-start = ((), (), s32[]{:S(2)}) async-start(), calls=%async_computation.2 | async-start | bytes 4194304 | tf_op jit(solution)/shard_map/psum | solution.py:171
  107.8 132.6 %all-gather.11.cloned.1.call-start = ((), (), s32[]{:S(2)}) async-start(), calls=%async_computation.3 | async-start | bytes 5242880 | tf_op jit(solution)/shard_map/all_gather | solution.py:177
  110.6 3.0 copy-start.3
  110.6 15.0 %copy-start.2 = (f32[1024]{0:T(1024)S(1)}, f32[1024]{0:T(1024)}, u32[]{:S(2)}) copy-start(f32[1024]{0:T(1024)} %param.27) | copy-start | bytes 12292
  110.6 210.5 %all-gather.13.cloned.1.call-start = ((), (), s32[]{:S(2)}) async-start(), calls=%async_computation.4 | async-start | bytes 5242880 | tf_op jit(solution)/shard_map/all_gather | solution.py:182
  113.6 267.5 %all-reduce.5.cloned.1.call-start = ((), (), s32[]{:S(2)}) async-start(), calls=%async_computation.5 | async-start | bytes 4194304 | tf_op jit(solution)/shard_map/psum | solution.py:185
  158.1 163.0 %copy-start.7 = (f32[2048]{0:T(1024)S(1)}, f32[2048]{0:T(1024)}, u32[]{:S(2)}) copy-start(f32[2048]{0:T(1024)} %param.25) | copy-start | bytes 24580
  331.0 0.7 copy-start.4
Sparse Core Ops, SparseCore 0:
  8.9 48.3 all-gather.6
  58.9 44.4 all-gather.8
  107.9 50.1 all-reduce.2
  159.6 80.8 all-gather.10
  241.8 79.2 all-gather.12
  331.2 49.8 all-reduce.4
